TPU v7x, 32 devices: a whole 2x2x4 slice. The times are simulated.
32 devices in a mesh: ep: 4 (over y, x), tp: 8 (over z, core).
Axes of the slice: x: 2, y: 2, z: 4, core: 2. Of those that a mesh axis runs over, the one named last changes fastest.
Arguments:
- tokens: bfloat16 [96, 4096], P('ep'), may hold values from -6 to 6
- norm_gain: float32 [4096], replicated, may hold values from 0.1 to 1.9
- w_query: bfloat16 [4096, 2048], P('ep', 'tp'), may hold values from -0.09375 to 0.09375
- w_forget: bfloat16 [4096, 2048], P('ep', 'tp'), may hold values from -0.09375 to 0.09375
- w_input: bfloat16 [4096, 2048], P('ep', 'tp'), may hold values from -0.09375 to 0.09375
- w_outgate: bfloat16 [4096, 2048], P('ep', 'tp'), may hold values from -0.09375 to 0.09375
- forget_floor: float32 [2048], P('tp'), may hold values from 0.3 to 0.95
- head_gain: float32 [2048], P('tp'), may hold values from 0.1 to 1.9
- recurrent_state: float32 [96, 16, 128, 128], P('ep', 'tp'), may hold values from -2.4 to 2.4
- w_output: bfloat16 [2048, 4096], P('tp', 'ep'), may hold values from -0.125 to 0.125
- ffn_gain: float32 [4096], replicated, may hold values from 0.1 to 1.9
- w_router: bfloat16 [4096, 8], replicated, may hold values from -0.09375 to 0.09375
- routes: int32 [96, 2], P('ep'), may hold values from 0 to 7, all different within a row; in each aligned block of 24 rows (0 to 23, 24 to 47, ...) at most 12 rows name the same one
- expert_gate: bfloat16 [8, 4096, 2816], P('ep', None, 'tp'), may hold values from -0.09375 to 0.09375
- expert_up: bfloat16 [8, 4096, 2816], P('ep', None, 'tp'), may hold values from -0.09375 to 0.09375
- expert_down: bfloat16 [8, 2816, 4096], P('ep', 'tp'), may hold values from -0.109375 to 0.109375
- shared_gate_w: bfloat16 [4096, 2816], P('ep', 'tp'), may hold values from -0.09375 to 0.09375
- shared_up_w: bfloat16 [4096, 2816], P('ep', 'tp'), may hold values from -0.09375 to 0.09375
- shared_down_w: bfloat16 [2816, 4096], P('tp', 'ep'), may hold values from -0.109375 to 0.109375
- branch_gate: bfloat16 [4096], replicated, may hold values from -0.09375 to 0.09375
Outputs:
- layer_out: bfloat16 [96, 4096], P('ep', 'tp')
- new_state: float32 [96, 16, 128, 128], P('ep', 'tp')
Inputs may be any that keep to these rules, and one draw needn't show every extreme that they name: `routes`: each row names 2 different experts. Among the rows of one index of ep, no expert is named more than 12 times, a bound that some block reaches.
All inputs are finite; a program needn't handle non-finite values.
Results may differ from a plain program's by a relative error of at most 0.025.
Values may be sent and summed in bfloat16 or wider, within the bound.
No kernel may reach another device: no remote copies, remote signals or barrier semaphores. Data moves between devices by JAX's collectives and lax.ppermute only.
A program may use at most 64 MiB of HBM per device.

v0:
```python
import jax
import jax.numpy as jnp
from jax import lax
from jax.sharding import PartitionSpec as P

NORM_EPSILON = 1e-06
ROUTED_SCALE = 2.5


def for_sending(array):
    return jax.tree.map(lambda a: a.astype(jnp.bfloat16) if a.dtype == jnp.float32 else a, array)


def rms_scale(values, gain):
    floats = values.astype(jnp.float32)
    inverse = lax.rsqrt(jnp.mean(floats * floats, axis=-1, keepdims=True) + NORM_EPSILON)
    return (floats * inverse * gain).astype(jnp.bfloat16)


def project(normed, weights):
    gathered = lax.all_to_all(normed, "ep", split_axis=1, concat_axis=0, tiled=True)
    terms = tuple(
        (jnp.dot(gathered, weight, preferred_element_type=jnp.float32) for weight in weights)
    )
    return jax.tree.map(
        lambda part: part.astype(jnp.float32),
        lax.psum_scatter(for_sending(terms), "ep", scatter_dimension=0, tiled=True),
    )


def expand(left, weight):
    return jnp.dot(
        left, lax.all_gather(weight, "ep", axis=1, tiled=True), preferred_element_type=jnp.float32
    )


def per_device(
    tokens,
    norm_gain,
    w_query,
    w_forget,
    w_input,
    w_outgate,
    forget_floor,
    head_gain,
    recurrent_state,
    w_output,
    ffn_gain,
    w_router,
    routes,
    expert_gate,
    expert_up,
    expert_down,
    shared_gate_w,
    shared_up_w,
    shared_down_w,
    branch_gate,
):
    batch, width = tokens.shape
    heads_here = recurrent_state.shape[1]
    head_size = recurrent_state.shape[2]
    normed = rms_scale(tokens, norm_gain)
    query, forget_pre, value_in, out_gate = project(normed, (w_query, w_forget, w_input, w_outgate))
    shape = (batch, heads_here, head_size)
    query = query.reshape(shape)
    forget_pre = forget_pre.reshape(shape)
    value_in = value_in.reshape(shape)
    floor = forget_floor.reshape(heads_here, head_size)
    forget = floor + (1.0 - floor) * jax.nn.sigmoid(forget_pre)
    key_part = (1.0 - floor) * jax.nn.sigmoid(-forget_pre)
    new_state = forget[..., None] * recurrent_state + key_part[..., None] * value_in[:, :, None, :]
    read = jnp.einsum(
        "bhk,bhkv->bhv", jax.nn.silu(query), new_state, precision=lax.Precision.HIGHEST
    )
    read = read * lax.rsqrt(jnp.mean(read * read, axis=-1, keepdims=True) + NORM_EPSILON)
    mixed_heads = (
        read.reshape(batch, heads_here * head_size) * head_gain * jax.nn.silu(out_gate)
    ).astype(jnp.bfloat16)
    mixer_out = lax.psum(expand(mixed_heads, w_output).astype(jnp.bfloat16), "tp").astype(
        jnp.float32
    )
    hidden = (tokens.astype(jnp.float32) + mixer_out).astype(jnp.bfloat16)
    normed_two = rms_scale(hidden, ffn_gain)
    experts = w_router.shape[1]
    top_count = routes.shape[1]
    capacity = max(2, 2 * batch * top_count // experts)
    affinity = jax.nn.sigmoid(jnp.dot(normed_two, w_router, preferred_element_type=jnp.float32))
    picks = routes[:, :, None] == jnp.arange(experts, dtype=jnp.int32)[None, None, :]
    chosen = jnp.sum(jnp.where(picks, affinity[:, None, :], 0.0), axis=2)
    route_weights = chosen / jnp.sum(chosen, axis=1, keepdims=True) * ROUTED_SCALE
    flat_routes = routes.reshape(-1)
    onehot = (flat_routes[:, None] == jnp.arange(experts, dtype=jnp.int32)[None, :]).astype(
        jnp.int32
    )
    earlier = jnp.cumsum(onehot, axis=0) - onehot
    slot = jnp.sum(earlier * onehot, axis=1)
    target = flat_routes * capacity + slot
    placing = target[:, None] == jnp.arange(experts * capacity, dtype=jnp.int32)[None, :]
    token_slot = jnp.sum(
        placing.reshape(batch, top_count, experts * capacity).astype(jnp.int32), axis=1
    )
    outgoing = jnp.dot(
        token_slot.astype(jnp.bfloat16).T, normed_two, preferred_element_type=jnp.float32
    )
    outgoing = outgoing.astype(jnp.bfloat16).reshape(experts, capacity, width)
    arrived = lax.all_to_all(outgoing, "ep", split_axis=0, concat_axis=1, tiled=True)
    gate_part = jnp.einsum("erd,edf->erf", arrived, expert_gate, preferred_element_type=jnp.float32)
    up_part = jnp.einsum("erd,edf->erf", arrived, expert_up, preferred_element_type=jnp.float32)
    inner = (jax.nn.silu(gate_part) * up_part).astype(jnp.bfloat16)
    expert_terms = jnp.einsum(
        "erf,efd->erd", inner, expert_down, preferred_element_type=jnp.float32
    )
    shared_gate, shared_up = project(normed_two, (shared_gate_w, shared_up_w))
    shared_inner = (jax.nn.silu(shared_gate) * shared_up).astype(jnp.bfloat16)
    shared_terms = expand(shared_inner, shared_down_w)
    local_experts = arrived.shape[0]
    expert_sums, shared_sums = (
        lax.psum_scatter(
            expert_terms.reshape(-1, width).astype(jnp.bfloat16),
            "tp",
            scatter_dimension=1,
            tiled=True,
        ).astype(jnp.float32),
        lax.psum_scatter(
            shared_terms.astype(jnp.bfloat16), "tp", scatter_dimension=1, tiled=True
        ).astype(jnp.float32),
    )
    slice_width = expert_sums.shape[1]
    returned = expert_sums.astype(jnp.bfloat16).reshape(local_experts, -1, slice_width)
    back = lax.all_to_all(returned, "ep", split_axis=1, concat_axis=0, tiled=True)
    per_route = jnp.dot(
        placing.astype(jnp.bfloat16),
        back.reshape(experts * capacity, slice_width),
        preferred_element_type=jnp.float32,
    )
    routed = jnp.sum(
        per_route.reshape(batch, top_count, slice_width) * route_weights[:, :, None], axis=1
    )
    branch = jax.nn.sigmoid(jnp.dot(normed_two, branch_gate, preferred_element_type=jnp.float32))
    offset = lax.axis_index("tp") * slice_width
    own_hidden = lax.dynamic_slice_in_dim(hidden, offset, slice_width, 1)
    layer_out = (own_hidden.astype(jnp.float32) + routed + branch[:, None] * shared_sums).astype(
        jnp.bfloat16
    )
    return (layer_out, new_state)


def solution(mesh):
    return jax.shard_map(
        per_device,
        mesh=mesh,
        in_specs=(
            P("ep", None),
            P(),
            P("ep", "tp"),
            P("ep", "tp"),
            P("ep", "tp"),
            P("ep", "tp"),
            P("tp"),
            P("tp"),
            P("ep", "tp", None, None),
            P("tp", "ep"),
            P(),
            P(),
            P("ep", None),
            P("ep", None, "tp"),
            P("ep", None, "tp"),
            P("ep", "tp", None),
            P("ep", "tp"),
            P("ep", "tp"),
            P("tp", "ep"),
            P(),
        ),
        out_specs=(P("ep", "tp"), P("ep", "tp", None, None)),
        check_vma=False,
    )
```

profile of v0, /device:TPU:0, one launch (start us, length us, event | category | flops | bytes accessed | tf_op | source)
XLA Modules:
  0.0 395.6 jit_solution(9614604141334358307)
XLA Ops:
  7.2 1.2 fusion.16
  8.4 1.1 fusion.18
  9.5 10.5 %all_to_all.71 = bf16[24,4,1024]{2,0,1:T(8,128)(2,1)S(1)} all-to-all(bf16[24,4,1024]{2,0,1:T(8,128)(2,1)S(1)} %bitcast.95), channel_id=1, replica_groups=mesh['ep'=4,'tp'=8] {'ep'}, dimensions={1} | all-to-all | bytes 393216 | tf_op jit(solution)/shard_map/all_to_all | solution.py:21
  20.0 1.9 convolution_convert_fusion.8
  22.0 1.9 convolution_convert_fusion.7
  24.0 1.9 convolution_convert_fusion.9
  27.5 17.7 %reduce-scatter.27.cloned.1.call-done = bf16[24,256]{1,0:T(8,128)(2,1)} async-done(((bf16[96,256]{1,0:T(8,128)(2,1)}), bf16[24,256]{1,0:T(8,128)(2,1)}) %reduce-scatter.27.cloned.1.call-update) | async-done | bytes 12304
  45.9 25.5 %reduce-scatter.29.cloned.1.call-done = bf16[24,256]{1,0:T(8,128)(2,1)} async-done(((bf16[96,256]{1,0:T(8,128)(2,1)}), bf16[24,256]{1,0:T(8,128)(2,1)}) %reduce-scatter.29.cloned.1.call-update) | async-done | bytes 12304
  72.1 26.1 %reduce-scatter.25.cloned.1.call-done = bf16[24,256]{1,0:T(8,128)(2,1)} async-done(((bf16[96,256]{1,0:T(8,128)(2,1)}), bf16[24,256]{1,0:T(8,128)(2,1)}) %reduce-scatter.25.cloned.1.call-update) | async-done | bytes 12304
  99.0 3.8 multiply_add_fusion
  102.8 1.6 copy-done.1
  104.5 2.8 fusion.55
  107.4 16.8 %reduce-scatter.31.cloned.1.call-done = bf16[24,256]{1,0:T(8,128)(2,1)} async-done(((bf16[96,256]{1,0:T(8,128)(2,1)}), bf16[24,256]{1,0:T(8,128)(2,1)}) %reduce-scatter.31.cloned.1.call-update) | async-done | bytes 12304
  124.3 36.9 %all-gather.3.cloned.1.call-done = bf16[256,4096]{1,0:T(8,128)(2,1)} async-done(((bf16[256,1024]{1,0:T(8,128)(2,1)}), bf16[256,4096]{1,0:T(8,128)(2,1)}) %all-gather.3.cloned.1.call-update) | async-done | bytes 2097168 | tf_op jit(solution)/shard_map/all_gather | solution.py:33
  161.2 2.7 convolution_convert_fusion.3
  164.0 55.3 %all-reduce.8.cloned.1.call-done = bf16[24,4096]{1,0:T(8,128)(2,1)} async-done(((bf16[24,4096]{1,0:T(8,128)(2,1)}), bf16[24,4096]{1,0:T(8,128)(2,1)}) %all-reduce.8.cloned.1.call-update) | async-done | bytes 196624 | tf_op jit(solution)/shard_map/psum | solution.py:79
  219.2 1.1 fusion.13
  220.5 9.0 %all_to_all.72 = bf16[24,4,1024]{2,0,1:T(8,128)(2,1)S(1)} all-to-all(bf16[24,4,1024]{2,0,1:T(8,128)(2,1)S(1)} %bitcast.96), channel_id=1, replica_groups=mesh['ep'=4,'tp'=8] {'ep'}, dimensions={1} | all-to-all | bytes 393216 | tf_op jit(solution)/shard_map/all_to_all | solution.py:21
  229.5 1.0 convolution_convert_fusion.5
  230.6 1.0 convolution_convert_fusion.4
  233.8 14.1 %all_to_all.73 = bf16[8,12,4096]{2,1,0:T(8,128)(2,1)S(1)} all-to-all(bf16[8,12,4096]{2,1,0:T(8,128)(2,1)S(1)} %reshape.164), channel_id=1, replica_groups=mesh['ep'=4,'tp'=8] {'ep'}, dimensions={0} | all-to-all | bytes 1572864 | tf_op jit(solution)/shard_map/all_to_all | solution.py:106
  248.7 4.6 %fusion.11 = f32[2,48,352]{2,1,0:T(8,128)S(1)} fusion(bf16[2,4096,352]{1,2,0:T(8,128)(2,1)} %param.33, bf16[2,48,4096]{2,0,1:T(2,128)(2,1)S(1)} %bitcast.83), kind=kOutput, calls=%fused_computation.25 | convolution fusion | flops 276824064 | bytes 6688768 | tf_op jit(solution)/shard_map/erd,edf->erf/dot_general | solution.py:107
  253.3 8.1 %convolution_convert_fusion = bf16[2,48,4096]{2,1,0:T(8,128)(2,1)} fusion(bf16[2,352,4096]{2,1,0:T(8,128)(2,1)} %param.35, bf16[2,4096,352]{1,2,0:T(8,128)(2,1)} %param.34, bf16[2,48,4096]{2,0,1:T(2,128)(2,1)S(1)} %bitcast.84, f32[2,48,352]{2,1,0:T(8,128)S(1)} %fusion.11), kind=kOutput, calls=%fused_computation | convolution fusion | flops 554244096 | bytes 13242368 | tf_op jit(solution)/shard_map/erf,efd->erd/dot_general | solution.py:110
  261.8 16.7 %reduce-scatter.35.cloned.1.call-done = bf16[24,352]{1,0:T(8,128)(2,1)} async-done(((bf16[96,352]{1,0:T(8,128)(2,1)}), bf16[24,352]{1,0:T(8,128)(2,1)}) %reduce-scatter.35.cloned.1.call-update) | async-done | bytes 16912
  278.6 43.6 %all-gather.5.cloned.1.call-done = bf16[352,4096]{1,0:T(8,128)(2,1)} async-done(((bf16[352,1024]{1,0:T(8,128)(2,1)}), bf16[352,4096]{1,0:T(8,128)(2,1)}) %all-gather.5.cloned.1.call-update) | async-done | bytes 2883600 | tf_op jit(solution)/shard_map/all_gather | solution.py:33
  322.1 3.1 convolution_convert_fusion.2
  325.2 30.9 %reduce-scatter.21.cloned.1.call-done = bf16[96,512]{1,0:T(8,128)(2,1)} async-done(((bf16[96,4096]{1,0:T(8,128)(2,1)}), bf16[96,512]{1,0:T(8,128)(2,1)}) %reduce-scatter.21.cloned.1.call-update) | async-done | bytes 98320 | tf_op jit(solution)/shard_map/reduce_scatter | solution.py:118
  356.1 1.6 copy.84
  357.7 3.8 all-to-all-start.2
  361.6 4.9 %all-to-all-done.2 = bf16[2,48,512]{2,0,1:T(2,128)(2,1)S(1)} async-done(((bf16[2,48,512]{2,0,1:T(2,128)(2,1)}), bf16[2,48,512]{2,0,1:T(2,128)(2,1)S(1)}, u32[]{:S(2)}, u32[]{:S(2)}) %all-to-all-start.2) | async-done | bytes 98336 | tf_op jit(solution)/shard_map/all_to_all | solution.py:130
  366.8 20.8 %reduce-scatter.23.cloned.1.call-done = bf16[24,512]{1,0:T(8,128)(2,1)} async-done(((bf16[24,4096]{1,0:T(8,128)(2,1)}), bf16[24,512]{1,0:T(8,128)(2,1)}) %reduce-scatter.23.cloned.1.call-update) | async-done | bytes 24592 | tf_op jit(solution)/shard_map/reduce_scatter | solution.py:124
  387.6 1.4 add_convert_fusion
  (83 shorter events, 8.2 us)
Async XLA Ops:
  7.2 222.3 %copy-start = (bf16[1024,352]{0,1:T(8,128)(2,1)S(1)}, bf16[1024,352]{0,1:T(8,128)(2,1)}, u32[]{:S(2)}) copy-start(bf16[1024,352]{0,1:T(8,128)(2,1)} %param.36) | copy-start | bytes 2162692
  7.2 18.7 %copy-start.4 = (bf16[1024,256]{1,0:T(8,128)(2,1)S(1)}, bf16[1024,256]{1,0:T(8,128)(2,1)}, u32[]{:S(2)}) copy-start(bf16[1024,256]{1,0:T(8,128)(2,1)} %param.25) | copy-start | bytes 1572868
  7.2 20.3 %copy-start.9 = (f32[256]{0:T(256)S(1)}, f32[256]{0:T(256)}, u32[]{:S(2)}) copy-start(f32[256]{0:T(256)} %param.26) | copy-start | bytes 3076
  7.2 37.9 %reduce-scatter.27.cloned.1.call-start = ((), (), s32[]{:S(2)}) async-start(), calls=%async_computation.18 | async-start | bytes 61440
  21.9 49.4 %reduce-scatter.29.cloned.1.call-start = ((), (), s32[]{:S(2)}) async-start(), calls=%async_computation.19 | async-start | bytes 61440
  23.9 74.3 %reduce-scatter.25.cloned.1.call-start = ((), (), s32[]{:S(2)}) async-start(), calls=%async_computation.17 | async-start | bytes 61440
  25.9 98.4 %reduce-scatter.31.cloned.1.call-start = ((), (), s32[]{:S(2)}) async-start(), calls=%async_computation.20 | async-start | bytes 61440
  26.8 134.4 %all-gather.3.cloned.1.call-start = ((), (), s32[]{:S(2)}) async-start(), calls=%async_computation.12 | async-start | bytes 2621440 | tf_op jit(solution)/shard_map/all_gather | solution.py:33
  27.4 191.8 %all-reduce.8.cloned.1.call-start = ((), (), s32[]{:S(2)}) async-start(), calls=%async_computation.13 | async-start | bytes 393216 | tf_op jit(solution)/shard_map/psum | solution.py:79
  102.8 1.7 copy-start.1
  102.8 58.4 %copy-start.10 = (f32[256]{0:T(256)S(1)}, f32[256]{0:T(256)}, u32[]{:S(2)}) copy-start(f32[256]{0:T(256)} %param.27) | copy-start | bytes 3076
  102.8 116.4 %copy-start.2 = (bf16[24,4096]{1,0:T(8,128)(2,1)S(1)}, bf16[24,4096]{1,0:T(8,128)(2,1)}, u32[]{:S(2)}) copy-start(bf16[24,4096]{1,0:T(8,128)(2,1)} %param.20) | copy-start | bytes 589828
  104.5 115.9 %copy-start.6 = (f32[4096]{0:T(1024)S(1)}, f32[4096]{0:T(1024)}, u32[]{:S(2)}) copy-start(f32[4096]{0:T(1024)} %param.30) | copy-start | bytes 49156
  107.2 123.3 %copy-start.3 = (bf16[1024,352]{0,1:T(8,128)(2,1)S(1)}, bf16[1024,352]{0,1:T(8,128)(2,1)}, u32[]{:S(2)}) copy-start(bf16[1024,352]{0,1:T(8,128)(2,1)} %param.37) | copy-start | bytes 2162692
  161.2 71.2 %copy-start.7 = (s32[24,2]{0,1:T(2,128)S(1)}, s32[24,2]{0,1:T(2,128)}, u32[]{:S(2)}) copy-start(s32[24,2]{0,1:T(2,128)} %param.32) | copy-start | bytes 580
  163.9 97.9 %reduce-scatter.33.cloned.1.call-start = ((), (), s32[]{:S(2)}) async-start(), calls=%async_computation.21 | async-start | bytes 92160
  230.5 48.1 %reduce-scatter.35.cloned.1.call-start = ((), (), s32[]{:S(2)}) async-start(), calls=%async_computation.22 | async-start | bytes 92160
  231.6 90.6 %all-gather.5.cloned.1.call-start = ((), (), s32[]{:S(2)}) async-start(), calls=%async_computation.15 | async-start | bytes 3604480 | tf_op jit(solution)/shard_map/all_gather | solution.py:33
  232.3 123.8 %reduce-scatter.21.cloned.1.call-start = ((), (), s32[]{:S(2)}) async-start(), calls=%async_computation.14 | async-start | bytes 884736 | tf_op jit(solution)/shard_map/reduce_scatter | solution.py:118
  253.2 8.2 %copy-start.8 = (bf16[4096]{0:T(1024)(128)(2,1)S(1)}, bf16[4096]{0:T(1024)(128)(2,1)}, u32[]{:S(2)}) copy-start(bf16[4096]{0:T(1024)(128)(2,1)} %param.39) | copy-start | bytes 24580
  253.2 8.4 %copy-start.5 = (bf16[4096,8]{0,1:T(8,128)(2,1)S(1)}, bf16[4096,8]{0,1:T(8,128)(2,1)}, u32[]{:S(2)}) copy-start(bf16[4096,8]{0,1:T(8,128)(2,1)} %param.31) | copy-start | bytes 196612
  261.4 126.2 %reduce-scatter.23.cloned.1.call-start = ((), (), s32[]{:S(2)}) async-start(), calls=%async_computation.16 | async-start | bytes 221184 | tf_op jit(solution)/shard_map/reduce_scatter | solution.py:124
  357.7 8.8 %all-to-all-start.2 = ((bf16[2,48,512]{2,0,1:T(2,128)(2,1)}), bf16[2,48,512]{2,0,1:T(2,128)(2,1)S(1)}, u32[]{:S(2)}, u32[]{:S(2)}) async-start(bf16[2,48,512]{2,0,1:T(2,128)(2,1)} %copy.84), calls=%async_computation.3 | async-start | bytes 196608 | tf_op jit(solution)/shard_map/all_to_all | solution.py:130
Sparse Core Ops, SparseCore 0:
  22.1 23.0 reduce-scatter.26
  47.9 23.4 reduce-scatter.28
  74.7 23.4 reduce-scatter.24
  100.8 23.4 reduce-scatter.30
  126.0 35.1 all-gather.2
  164.0 55.1 all-reduce.7
  230.6 21.5 reduce-scatter.32
  255.0 23.5 reduce-scatter.34
  280.4 41.6 all-gather.4
  324.3 31.8 reduce-scatter.20
  358.4 29.1 reduce-scatter.22
where the time goes:
time: 397 us; the launch traced here: 396 us
  waiting for transfers between devices  297 us (75%)
  blocking collectives  33.6 us (8%)
  matrix products  30.6 us (8%)
  between operations  14.2 us (4%)
  other arithmetic  10.1 us (3%)
  local copies, waits for them, and re-layouts  6.22 us (2%)
  starting transfers between devices  4.3 us (1%)
    unnamed x17, waiting for transfers between devices  104 us
    all_gather x2, waiting for transfers between devices, expand(): lax.all_gather(weight, 'ep', axis=1, tiled=True)  80.5 us
    psum x1, waiting for transfers between devices, per_device(): lax.psum(expand(mixed_heads, w_output).astype(jnp.bfloat16), 'tp')  55.3 us
    reduce_scatter x1, waiting for transfers between devices, per_device(): lax.psum_scatter(expert_terms.reshape(-1, width).astype(jnp.bfloat16), 't...  30.9 us
    reduce_scatter x1, waiting for transfers between devices, per_device(): lax.psum_scatter(shared_terms.astype(jnp.bfloat16), 'tp', scatter_dimensi...  20.8 us
    all_to_all x2, blocking collectives, project(): lax.all_to_all(normed, 'ep', split_axis=1, concat_axis=0, tiled=True)  19.5 us
    all_to_all x1, blocking collectives, per_device(): lax.all_to_all(outgoing, 'ep', split_axis=0, concat_axis=1, tiled=True)  14.1 us
    dot_general x6, matrix products, project(): jnp.dot(gathered, weight, preferred_element_type=jnp.float32)  8.48 us
  transfers between devices with their start and end apart: 12, of which 11 were waited for; matrix products, arithmetic and copies ran while one was open for 9% of the time, Pallas kernels for 0%

commit v1 on v0

--- a/solution.py
+++ b/solution.py
@@ -76,9 +76,9 @@
     mixed_heads = (
         read.reshape(batch, heads_here * head_size) * head_gain * jax.nn.silu(out_gate)
     ).astype(jnp.bfloat16)
-    mixer_out = lax.psum(expand(mixed_heads, w_output).astype(jnp.bfloat16), "tp").astype(
-        jnp.float32
-    )
+    mixer_out = jnp.sum(
+        lax.all_gather(expand(mixed_heads, w_output).astype(jnp.bfloat16), "tp"), axis=0
+    ).astype(jnp.float32)
     hidden = (tokens.astype(jnp.float32) + mixer_out).astype(jnp.bfloat16)
     normed_two = rms_scale(hidden, ffn_gain)
     experts = w_router.shape[1]

time: 397 us -> 368 us (0.927)
  blocking collectives: 33.6 us -> 10.5 us
  waiting for transfers between devices: 297 us -> 281 us
  starting transfers between devices: 4.3 us -> 11.4 us
    psum x1 -> x0, waiting for transfers between devices: 55.3 us -> none  [per_device(): lax.psum(expand(mixed_heads, w_output).astype(jnp.bfloat16), 'tp')]
    all_gather x2, waiting for transfers between devices: 80.5 us -> 44.1 us  [expand(): lax.all_gather(weight, 'ep', axis=1, tiled=True)]
    unnamed x17, waiting for transfers between devices: 104 us -> 140 us
    all_gather x0 -> x1, waiting for transfers between devices: none -> 23.9 us  [per_device(): lax.all_gather(expand(mixed_heads, w_output).astype(jnp.bfloat16), 'tp')]
    all_to_all x0 -> x2, waiting for transfers between devices: none -> 15.9 us  [the longest x1 12.2 us: per_device(): lax.all_to_all(outgoing, 'ep', split_axis=0, concat_axis=1, tiled=True)]
    all_to_all x1 -> x0, blocking collectives: 14.1 us -> none  [per_device(): lax.all_to_all(outgoing, 'ep', split_axis=0, concat_axis=1, tiled=True)]
    all_to_all x2 -> x1, blocking collectives: 19.5 us -> 10.5 us  [project(): lax.all_to_all(normed, 'ep', split_axis=1, concat_axis=0, tiled=True)]
    all_to_all x0 -> x2, starting transfers between devices: none -> 7.16 us  [the longest x1 3.65 us: project(): lax.all_to_all(normed, 'ep', split_axis=1, concat_axis=0, tiled=True)]
  transfers between devices with their start and end apart: 12 -> 14, of which waited for: 11 -> 14; matrix products, arithmetic and copies ran while one was open for 9% -> 11% of each run, Pallas kernels for 0% -> 0%
where the time goes in v1:
time: 368 us; the launch traced here: 367 us
  waiting for transfers between devices  281 us (76%)
  matrix products  31.7 us (9%)
  between operations  14.2 us (4%)
  starting transfers between devices  11.4 us (3%)
  other arithmetic  10.8 us (3%)
  blocking collectives  10.5 us (3%)
  local copies, waits for them, and re-layouts  7.87 us (2%)
    unnamed x17, waiting for transfers between devices  140 us
    all_gather x2, waiting for transfers between devices, expand(): lax.all_gather(weight, 'ep', axis=1, tiled=True)  44.1 us
    reduce_scatter x1, waiting for transfers between devices, per_device(): lax.psum_scatter(expert_terms.reshape(-1, width).astype(jnp.bfloat16), 't...  30.9 us
    all_gather x1, waiting for transfers between devices, per_device(): lax.all_gather(expand(mixed_heads, w_output).astype(jnp.bfloat16), 'tp')  23.9 us
    reduce_scatter x1, waiting for transfers between devices, per_device(): lax.psum_scatter(shared_terms.astype(jnp.bfloat16), 'tp', scatter_dimensi...  20.9 us
    all_to_all x1, waiting for transfers between devices, per_device(): lax.all_to_all(outgoing, 'ep', split_axis=0, concat_axis=1, tiled=True)  12.2 us
    all_to_all x1, blocking collectives, project(): lax.all_to_all(normed, 'ep', split_axis=1, concat_axis=0, tiled=True)  10.5 us
    dot_general x6, matrix products, project(): jnp.dot(gathered, weight, preferred_element_type=jnp.float32)  9.59 us
  transfers between devices with their start and end apart: 14, of which 14 were waited for; matrix products, arithmetic and copies ran while one was open for 11% of the time, Pallas kernels for 0%

profile of v1, /device:TPU:0, one launch (start us, length us, event | category | flops | bytes accessed | tf_op | source)
XLA Modules:
  0.0 367.2 jit_solution(17822848806876918838)
XLA Ops:
  9.5 10.5 %all_to_all.71 = bf16[24,4,1024]{2,0,1:T(8,128)(2,1)S(1)} all-to-all(bf16[24,4,1024]{2,0,1:T(8,128)(2,1)S(1)} %bitcast.97), channel_id=1, replica_groups=mesh['ep'=4,'tp'=8] {'ep'}, dimensions={1} | all-to-all | bytes 393216 | tf_op jit(solution)/shard_map/all_to_all | solution.py:21
  20.0 1.9 convolution_convert_fusion.8
  22.0 1.9 convolution_convert_fusion.7
  24.0 1.9 convolution_convert_fusion.9
  27.5 17.7 %reduce-scatter.27.cloned.1.call-done = bf16[24,256]{1,0:T(8,128)(2,1)} async-done(((bf16[96,256]{1,0:T(8,128)(2,1)}), bf16[24,256]{1,0:T(8,128)(2,1)}) %reduce-scatter.27.cloned.1.call-update) | async-done | bytes 12304
  45.9 25.5 %reduce-scatter.29.cloned.1.call-done = bf16[24,256]{1,0:T(8,128)(2,1)} async-done(((bf16[96,256]{1,0:T(8,128)(2,1)}), bf16[24,256]{1,0:T(8,128)(2,1)}) %reduce-scatter.29.cloned.1.call-update) | async-done | bytes 12304
  72.1 26.1 %reduce-scatter.25.cloned.1.call-done = bf16[24,256]{1,0:T(8,128)(2,1)} async-done(((bf16[96,256]{1,0:T(8,128)(2,1)}), bf16[24,256]{1,0:T(8,128)(2,1)}) %reduce-scatter.25.cloned.1.call-update) | async-done | bytes 12304
  99.0 3.8 %multiply_add_fusion = f32[24,2,128,128]{3,2,1,0:T(8,128)S(1)} fusion(f32[24,2,128,128]{3,2,1,0:T(8,128)} %param.28, f32[24,2,128]{2,1,0:T(2,128)S(1)} %reshape.169, f32[24,2,128]{2,1,0:T(2,128)S(1)} %bitcast.104, f32[24,2,128]{2,1,0:T(2,128)S(1)} %bitcast.103), kind=kLoop, calls=%fused_computation.4 | loop fusion | flops 2359296 | bytes 6365184 | tf_op jit(solution)/shard_map/add | solution.py:71
  102.8 1.6 copy-done.1
  104.5 2.8 fusion.55
  107.4 16.9 %reduce-scatter.31.cloned.1.call-done = bf16[24,256]{1,0:T(8,128)(2,1)} async-done(((bf16[96,256]{1,0:T(8,128)(2,1)}), bf16[24,256]{1,0:T(8,128)(2,1)}) %reduce-scatter.31.cloned.1.call-update) | async-done | bytes 12304
  124.3 36.9 %all-gather.5.cloned.1.call-done = bf16[256,4096]{1,0:T(8,128)(2,1)} async-done(((bf16[256,1024]{1,0:T(8,128)(2,1)}), bf16[256,4096]{1,0:T(8,128)(2,1)}) %all-gather.5.cloned.1.call-update) | async-done | bytes 2097168 | tf_op jit(solution)/shard_map/all_gather | solution.py:33
  161.2 2.7 convolution_convert_fusion.3
  165.4 23.9 %all-gather.9.cloned.1.call-done = bf16[192,4096]{1,0:T(8,128)(2,1)} async-done(((bf16[24,4096]{1,0:T(8,128)(2,1)}), bf16[192,4096]{1,0:T(8,128)(2,1)}) %all-gather.9.cloned.1.call-update) | async-done | bytes 1572880 | tf_op jit(solution)/shard_map/all_gather | solution.py:80
  189.4 1.7 reduce_sum.88
  192.1 3.6 all-to-all-start.3
  197.2 3.7 %all-to-all-done.3 = bf16[24,4,1024]{2,0,1:T(8,128)(2,1)S(1)} async-done(((bf16[24,4,1024]{2,0,1:T(8,128)(2,1)}), bf16[24,4,1024]{2,0,1:T(8,128)(2,1)S(1)}, u32[]{:S(2)}, u32[]{:S(2)}) %all-to-all-start.3) | async-done | bytes 196640 | tf_op jit(solution)/shard_map/all_to_all | solution.py:21
  200.9 3.5 all-to-all-start.1
  205.6 2.1 convolution_convert_fusion.4
  207.7 12.2 %all-to-all-done.1 = bf16[8,12,4096]{2,1,0:T(8,128)(2,1)S(1)} async-done(((bf16[8,12,4096]{2,1,0:T(8,128)(2,1)}), bf16[8,12,4096]{2,1,0:T(8,128)(2,1)S(1)}, u32[]{:S(2)}, u32[]{:S(2)}) %all-to-all-start.1) | async-done | bytes 786464 | tf_op jit(solution)/shard_map/all_to_all | solution.py:106
  220.8 4.6 %fusion.11 = f32[2,48,352]{2,1,0:T(8,128)S(1)} fusion(bf16[2,4096,352]{1,2,0:T(8,128)(2,1)} %param.33, bf16[2,48,4096]{2,0,1:T(2,128)(2,1)S(1)} %bitcast.84), kind=kOutput, calls=%fused_computation.25 | convolution fusion | flops 276824064 | bytes 6688768 | tf_op jit(solution)/shard_map/erd,edf->erf/dot_general | solution.py:107
  225.4 8.1 %convolution_convert_fusion = bf16[2,48,4096]{2,1,0:T(8,128)(2,1)} fusion(bf16[2,352,4096]{2,1,0:T(8,128)(2,1)} %param.35, bf16[2,4096,352]{1,2,0:T(8,128)(2,1)} %param.34, bf16[2,48,4096]{2,0,1:T(2,128)(2,1)S(1)} %bitcast.85, f32[2,48,352]{2,1,0:T(8,128)S(1)} %fusion.11), kind=kOutput, calls=%fused_computation | convolution fusion | flops 554244096 | bytes 13242368 | tf_op jit(solution)/shard_map/erf,efd->erd/dot_general | solution.py:110
  234.0 7.2 %all-gather.7.cloned.1.call-done = bf16[352,4096]{1,0:T(8,128)(2,1)} async-done(((bf16[352,1024]{1,0:T(8,128)(2,1)}), bf16[352,4096]{1,0:T(8,128)(2,1)}) %all-gather.7.cloned.1.call-update) | async-done | bytes 2883600 | tf_op jit(solution)/shard_map/all_gather | solution.py:33
  241.2 26.3 %reduce-scatter.33.cloned.1.call-done = bf16[24,352]{1,0:T(8,128)(2,1)} async-done(((bf16[96,352]{1,0:T(8,128)(2,1)}), bf16[24,352]{1,0:T(8,128)(2,1)}) %reduce-scatter.33.cloned.1.call-update) | async-done | bytes 16912
  267.4 26.3 %reduce-scatter.35.cloned.1.call-done = bf16[24,352]{1,0:T(8,128)(2,1)} async-done(((bf16[96,352]{1,0:T(8,128)(2,1)}), bf16[24,352]{1,0:T(8,128)(2,1)}) %reduce-scatter.35.cloned.1.call-update) | async-done | bytes 16912
  293.8 3.1 convolution_convert_fusion.2
  296.9 30.9 %reduce-scatter.21.cloned.1.call-done = bf16[96,512]{1,0:T(8,128)(2,1)} async-done(((bf16[96,4096]{1,0:T(8,128)(2,1)}), bf16[96,512]{1,0:T(8,128)(2,1)}) %reduce-scatter.21.cloned.1.call-update) | async-done | bytes 98320 | tf_op jit(solution)/shard_map/reduce_scatter | solution.py:118
  327.8 1.6 copy.84
  329.4 3.8 %all-to-all-start.2 = ((bf16[2,48,512]{2,0,1:T(2,128)(2,1)}), bf16[2,48,512]{2,0,1:T(2,128)(2,1)S(1)}, u32[]{:S(2)}, u32[]{:S(2)}) async-start(bf16[2,48,512]{2,0,1:T(2,128)(2,1)} %copy.84), calls=%async_computation.3 | async-start | bytes 196608 | tf_op jit(solution)/shard_map/all_to_all | solution.py:130
  333.2 4.9 %all-to-all-done.2 = bf16[2,48,512]{2,0,1:T(2,128)(2,1)S(1)} async-done(((bf16[2,48,512]{2,0,1:T(2,128)(2,1)}), bf16[2,48,512]{2,0,1:T(2,128)(2,1)S(1)}, u32[]{:S(2)}, u32[]{:S(2)}) %all-to-all-start.2) | async-done | bytes 98336 | tf_op jit(solution)/shard_map/all_to_all | solution.py:130
  338.4 20.9 %reduce-scatter.23.cloned.1.call-done = bf16[24,512]{1,0:T(8,128)(2,1)} async-done(((bf16[24,4096]{1,0:T(8,128)(2,1)}), bf16[24,512]{1,0:T(8,128)(2,1)}) %reduce-scatter.23.cloned.1.call-update) | async-done | bytes 24592 | tf_op jit(solution)/shard_map/reduce_scatter | solution.py:124
  359.3 1.4 add_convert_fusion
  (84 shorter events, 13.2 us)
Async XLA Ops:
  7.2 197.3 %copy-start = (bf16[1024,352]{0,1:T(8,128)(2,1)S(1)}, bf16[1024,352]{0,1:T(8,128)(2,1)}, u32[]{:S(2)}) copy-start(bf16[1024,352]{0,1:T(8,128)(2,1)} %param.36) | copy-start | bytes 2162692
  7.2 18.7 %copy-start.3 = (bf16[1024,256]{1,0:T(8,128)(2,1)S(1)}, bf16[1024,256]{1,0:T(8,128)(2,1)}, u32[]{:S(2)}) copy-start(bf16[1024,256]{1,0:T(8,128)(2,1)} %param.25) | copy-start | bytes 1572868
  7.2 20.3 %copy-start.8 = (f32[256]{0:T(256)S(1)}, f32[256]{0:T(256)}, u32[]{:S(2)}) copy-start(f32[256]{0:T(256)} %param.26) | copy-start | bytes 3076
  7.2 37.9 %reduce-scatter.27.cloned.1.call-start = ((), (), s32[]{:S(2)}) async-start(), calls=%async_computation.18 | async-start | bytes 61440
  21.9 49.4 %reduce-scatter.29.cloned.1.call-start = ((), (), s32[]{:S(2)}) async-start(), calls=%async_computation.19 | async-start | bytes 61440
  23.9 74.3 %reduce-scatter.25.cloned.1.call-start = ((), (), s32[]{:S(2)}) async-start(), calls=%async_computation.17 | async-start | bytes 61440
  25.9 98.4 %reduce-scatter.31.cloned.1.call-start = ((), (), s32[]{:S(2)}) async-start(), calls=%async_computation.20 | async-start | bytes 61440
  26.8 134.4 %all-gather.5.cloned.1.call-start = ((), (), s32[]{:S(2)}) async-start(), calls=%async_computation.12 | async-start | bytes 2621440 | tf_op jit(solution)/shard_map/all_gather | solution.py:33
  27.4 162.0 %all-gather.9.cloned.1.call-start = ((), (), s32[]{:S(2)}) async-start(), calls=%async_computation.16 | async-start | bytes 1769472 | tf_op jit(solution)/shard_map/all_gather | solution.py:80
  102.8 1.7 copy-start.1
  102.8 58.4 %copy-start.9 = (f32[256]{0:T(256)S(1)}, f32[256]{0:T(256)}, u32[]{:S(2)}) copy-start(f32[256]{0:T(256)} %param.27) | copy-start | bytes 3076
  104.5 60.2 %copy-start.6 = (s32[24,2]{0,1:T(2,128)S(1)}, s32[24,2]{0,1:T(2,128)}, u32[]{:S(2)}) copy-start(s32[24,2]{0,1:T(2,128)} %param.32) | copy-start | bytes 580
  107.2 83.8 %copy-start.2 = (bf16[24,4096]{1,0:T(8,128)(2,1)S(1)}, bf16[24,4096]{1,0:T(8,128)(2,1)}, u32[]{:S(2)}) copy-start(bf16[24,4096]{1,0:T(8,128)(2,1)} %param.20) | copy-start | bytes 589828
  107.2 84.0 %copy-start.5 = (f32[4096]{0:T(1024)S(1)}, f32[4096]{0:T(1024)}, u32[]{:S(2)}) copy-start(f32[4096]{0:T(1024)} %param.30) | copy-start | bytes 49156
  163.9 77.3 %all-gather.7.cloned.1.call-start = ((), (), s32[]{:S(2)}) async-start(), calls=%async_computation.14 | async-start | bytes 3604480 | tf_op jit(solution)/shard_map/all_gather | solution.py:33
  192.1 8.9 %all-to-all-start.3 = ((bf16[24,4,1024]{2,0,1:T(8,128)(2,1)}), bf16[24,4,1024]{2,0,1:T(8,128)(2,1)S(1)}, u32[]{:S(2)}, u32[]{:S(2)}) async-start(bf16[24,4,1024]{2,0,1:T(8,128)(2,1)} %bitcast.76), calls=%async_computation.4 | async-start | bytes 393216 | tf_op jit(solution)/shard_map/all_to_all | solution.py:21
  200.9 19.0 %all-to-all-start.1 = ((bf16[8,12,4096]{2,1,0:T(8,128)(2,1)}), bf16[8,12,4096]{2,1,0:T(8,128)(2,1)S(1)}, u32[]{:S(2)}, u32[]{:S(2)}) async-start(bf16[8,12,4096]{2,1,0:T(8,128)(2,1)} %reshape.164), calls=%async_computation.1 | async-start | bytes 2097152 | tf_op jit(solution)/shard_map/all_to_all | solution.py:106
  204.5 63.0 %reduce-scatter.33.cloned.1.call-start = ((), (), s32[]{:S(2)}) async-start(), calls=%async_computation.21 | async-start | bytes 92160
  205.5 88.2 %reduce-scatter.35.cloned.1.call-start = ((), (), s32[]{:S(2)}) async-start(), calls=%async_computation.22 | async-start | bytes 92160
  207.7 120.1 %reduce-scatter.21.cloned.1.call-start = ((), (), s32[]{:S(2)}) async-start(), calls=%async_computation.13 | async-start | bytes 884736 | tf_op jit(solution)/shard_map/reduce_scatter | solution.py:118
  225.3 8.2 %copy-start.7 = (bf16[4096]{0:T(1024)(128)(2,1)S(1)}, bf16[4096]{0:T(1024)(128)(2,1)}, u32[]{:S(2)}) copy-start(bf16[4096]{0:T(1024)(128)(2,1)} %param.39) | copy-start | bytes 24580
  225.4 8.4 %copy-start.4 = (bf16[4096,8]{0,1:T(8,128)(2,1)S(1)}, bf16[4096,8]{0,1:T(8,128)(2,1)}, u32[]{:S(2)}) copy-start(bf16[4096,8]{0,1:T(8,128)(2,1)} %param.31) | copy-start | bytes 196612
  233.5 125.8 %reduce-scatter.23.cloned.1.call-start = ((), (), s32[]{:S(2)}) async-start(), calls=%async_computation.15 | async-start | bytes 221184 | tf_op jit(solution)/shard_map/reduce_scatter | solution.py:124
  329.4 8.7 %all-to-all-start.2 = ((bf16[2,48,512]{2,0,1:T(2,128)(2,1)}), bf16[2,48,512]{2,0,1:T(2,128)(2,1)S(1)}, u32[]{:S(2)}, u32[]{:S(2)}) async-start(bf16[2,48,512]{2,0,1:T(2,128)(2,1)} %copy.84), calls=%async_computation.3 | async-start | bytes 196608 | tf_op jit(solution)/shard_map/all_to_all | solution.py:130
Sparse Core Ops, SparseCore 0:
  22.1 23.0 reduce-scatter.26
  47.9 23.4 reduce-scatter.28
  74.7 23.4 reduce-scatter.24
  100.8 23.4 reduce-scatter.30
  126.0 35.1 all-gather.4
  164.0 25.3 all-gather.8
  191.2 49.9 all-gather.6
  243.9 23.5 reduce-scatter.32
  270.2 23.5 reduce-scatter.34
  295.9 31.8 reduce-scatter.20
  330.0 29.2 reduce-scatter.22
